TPU v7x, 512 devices: a whole 4x8x8 slice. The times are simulated.
512 devices in a mesh: sp: 128 (over z, y, core), tp: 4 (over x).
Axes of the slice: x: 4, y: 8, z: 8, core: 2. Of those that a mesh axis runs over, the one named last changes fastest.
Arguments:
- tokens: bfloat16 [65536, 2048], P(('sp', 'tp')), may hold values from -6 to 6
- pooling_input_weight: bfloat16 [2048, 1024], P('sp', 'tp'), may hold values from -0.125 to 0.125
- query_matrix: bfloat16 [2048, 512], P('sp', 'tp'), may hold values from -0.125 to 0.125
- key_matrix: bfloat16 [2048, 512], P('sp', 'tp'), may hold values from -0.125 to 0.125
- value_matrix: bfloat16 [2048, 1024], P('sp', 'tp'), may hold values from -0.125 to 0.125
- decay_inner_weight: bfloat16 [2048, 64], replicated, may hold values from -0.125 to 0.125
- decay_outer_weight: bfloat16 [2, 32, 512], replicated, may hold values from -1 to 1
- channel_decay_bias: float32 [2, 512], replicated, may hold values from -0.3 to 12
- spike_log_decay: float32 [8, 65536], P('tp', 'sp'), may hold values from -0.72 to 0
- starting_state: float32 [2, 8, 64, 128], P(None, 'tp'), may hold values from -1536 to 1536
- pooling_group_map: bfloat16 [4, 256, 256], replicated, may hold values from -0.375 to 0.375
- pooling_output_weight: bfloat16 [1024, 2048], P('tp', 'sp'), may hold values from -0.125 to 0.125
- attention_output_weight: bfloat16 [1024, 2048], P('tp', 'sp'), may hold values from -0.125 to 0.125
Outputs:
- mixed: bfloat16 [65536, 2048], P(('sp', 'tp'))
All inputs are finite; a program needn't handle non-finite values.
Results may differ from a plain program's by a relative error of at most 0.015.
Values may be sent and summed in bfloat16 or wider, within the bound.
No kernel may reach another device: no remote copies, remote signals or barrier semaphores. Data moves between devices by JAX's collectives and lax.ppermute only.
A program may use at most 64 MiB of HBM per device.

v0:
```python
import jax
import jax.numpy as jnp
from jax import lax
from jax.sharding import Mesh
from jax.sharding import PartitionSpec as P

KEY_CHANNELS = 64
DV = 128
RANK = 32
BLOCK = 64
SP = ("sp_0", "sp_1", "sp_2")
SP_TP = ("sp_0", "sp_1", "sp_2", "tp")
eps_value = 1e-06
gate_norm_factor = 16.0
rim_width = 8


def from_everyone(value, axis):
    copies = jnp.broadcast_to(value, (lax.axis_size(axis), *value.shape))
    return lax.all_to_all(copies, axis, split_axis=0, concat_axis=0, tiled=True)


def laid_out(tiles, dim):
    tiles = jnp.moveaxis(tiles, 0, dim)
    lengths = tiles.shape
    return tiles.reshape(*lengths[:dim], lengths[dim] * lengths[dim + 1], *lengths[dim + 2 :])


def gathered_copies(value, axis, dim):
    tiles = from_everyone(value, axis)
    return laid_out(tiles, dim)


def extended(value, sides, width):
    for axis, dim in sides:
        devices, length = (lax.axis_size(axis), value.shape[dim])
        up = [(i, (i + 1) % devices) for i in range(devices - 1)]
        down = [(j, i) for i, j in up]
        last = lax.slice_in_dim(value, length - width, length, axis=dim)
        leading = lax.slice_in_dim(value, 0, width, axis=dim)
        before = lax.ppermute(last, axis, up)
        after = lax.ppermute(leading, axis, down)
        value = jnp.concatenate([before, value, after], axis=dim)
    return value


def neutral_like(value, identity):
    return jax.tree.map(
        lambda a, e: jnp.broadcast_to(jnp.asarray(e, a.dtype), a.shape), value, identity
    )


def carried_in(value, axes, combine, identity):
    before = start = neutral_like(value, identity)
    total = value
    for axis in reversed(axes):
        devices, mine = (lax.axis_size(axis), lax.axis_index(axis))
        pieces = jax.tree.map(
            lambda part, kind: lax.all_gather(part.astype(kind), axis),
            total,
            jax.tree.map(lambda a: jnp.bfloat16 if a.dtype == jnp.float32 else a.dtype, value),
        )
        inside, total = (start, start)
        for k in range(devices):
            passed = k < mine
            total = combine(
                total, jax.tree.map(lambda part, own: part[k].astype(own.dtype), pieces, value)
            )
            inside = jax.tree.map(lambda new, old: jnp.where(passed, new, old), total, inside)
        before = combine(inside, before)
    return before


def gathered_once(value, axis):
    leaves = jax.tree.leaves(value)
    order = sorted(range(len(leaves)), key=lambda k: -leaves[k].size)
    width = (1, *leaves[order[0]].shape)[-1]
    lines = [
        jnp.pad(leaves[k].reshape(-1), (0, -leaves[k].size % width)).reshape(-1, width)
        for k in order
    ]
    both, at, found = (lax.all_gather(jnp.concatenate(lines), axis), 0, {})
    for k, line in zip(order, lines):
        section = both[:, at : at + len(line)].reshape(len(both), -1)
        found[k] = section[:, : leaves[k].size].reshape(-1, *leaves[k].shape)
        at += len(line)
    numbers = iter(range(len(leaves)))
    return jax.tree.map(lambda _: found[next(numbers)], value)


def carried_in_2(value, axes, combine, identity):
    before = start = neutral_like(value, identity)
    total = value
    for axis in reversed(axes):
        devices, mine = (lax.axis_size(axis), lax.axis_index(axis))
        pieces = gathered_once(
            jax.tree.map(
                lambda part, kind: part.astype(kind),
                total,
                jax.tree.map(lambda a: jnp.bfloat16 if a.dtype == jnp.float32 else a.dtype, value),
            ),
            axis,
        )
        inside, total = (start, start)
        for k in reversed(range(devices)):
            passed = k > mine
            total = combine(
                total, jax.tree.map(lambda part, own: part[k].astype(own.dtype), pieces, value)
            )
            inside = jax.tree.map(lambda new, old: jnp.where(passed, new, old), total, inside)
        before = combine(inside, before)
    return before


def gather_turned(arrays, axis, dims):
    turned = [jnp.moveaxis(a, dim, 0) for a, dim in zip(arrays, dims)]
    both = jnp.concatenate([t.reshape(len(t), -1) for t in turned], axis=1)
    filled, at, finished = (lax.all_gather(both, axis, axis=0, tiled=True), 0, [])
    for t, dim in zip(turned, dims):
        section = filled[:, at : at + t[0].size].reshape(-1, *t.shape[1:])
        finished.append(jnp.moveaxis(section, 0, dim))
        at += t[0].size
    return tuple(finished)


def cut_along(value, dim, devices):
    lengths = value.shape
    tiles = value.reshape(*lengths[:dim], devices, lengths[dim] // devices, *lengths[dim + 1 :])
    return jnp.moveaxis(tiles, dim, 0)


def sum_at_owner(value, axis, dim):
    devices = lax.axis_size(axis)
    tiles = lax.all_to_all(cut_along(value, dim, devices), axis, 0, 0, tiled=True)
    return jnp.sum(tiles.astype(jnp.float32), axis=0)


def normalize(token_rows):
    floats = token_rows.astype(jnp.float32)
    scaled = floats * lax.rsqrt(jnp.mean(floats * floats, axis=-1, keepdims=True) + eps_value)
    return scaled.astype(jnp.bfloat16)


def chain_combine(earlier, later):
    return (earlier[0] + later[0], jnp.exp(later[0])[..., None] * earlier[1] + later[1])


def local_chain(decays, updates, backward):

    def advance(carried, element):
        log_total, memory = carried
        decay_now, update_now = element
        return (
            (log_total + decay_now, jnp.exp(decay_now)[..., None] * memory + update_now),
            (log_total, memory),
        )

    begin = (jnp.zeros_like(decays[0]), jnp.zeros_like(updates[0]))
    return lax.scan(advance, begin, (decays, updates), reverse=backward)


def within_blocks(queries, cumulative, key_rows, value_rows, lower):
    row_ids = lax.broadcasted_iota(jnp.int32, (BLOCK, BLOCK), 0)
    col_ids = lax.broadcasted_iota(jnp.int32, (BLOCK, BLOCK), 1)
    allowed = col_ids <= row_ids if lower else col_ids > row_ids
    scaled_q = queries * jnp.exp(cumulative)
    scaled_k = key_rows * jnp.exp(-cumulative)
    scores = jnp.einsum("hnid,hnjd->hnij", scaled_q, scaled_k)
    scores = jnp.where(allowed, scores, 0.0)
    return (scaled_q, jnp.einsum("hnij,hnjv->hniv", scores, value_rows))


def block_updates(key_rows, value_rows, cumulative, edge):
    weighted = key_rows * jnp.exp(edge[:, :, None, :] - cumulative)
    return jnp.einsum("hncd,hncv->hndv", weighted, value_rows)


def carried_term(scaled_q, before, entering):
    log_before, memory_before = before
    block_memory = jnp.exp(log_before)[..., None] * entering[None] + memory_before
    return jnp.einsum("hnid,nhdv->hniv", scaled_q, block_memory)


def shards(
    tokens,
    pooling_input_weight,
    query_matrix,
    key_matrix,
    value_matrix,
    decay_inner_weight,
    decay_outer_weight,
    channel_decay_bias,
    spike_log_decay,
    starting_state,
    pooling_group_map,
    pooling_output_weight,
    attention_output_weight,
):
    sp_index = lax.axis_index(SP)
    tp_index = lax.axis_index("tp")
    normed = normalize(tokens)
    pool_cols = pooling_input_weight.shape[1]
    qk_cols = query_matrix.shape[1]
    value_cols = value_matrix.shape[1]
    local_weight = jnp.concatenate(
        [pooling_input_weight, query_matrix, key_matrix, value_matrix], axis=1
    )
    all_rows = gathered_copies(normed, "tp", 0)
    summed = jnp.dot(
        all_rows,
        lax.all_gather(local_weight, SP, axis=0, tiled=True),
        preferred_element_type=jnp.float32,
    )
    rank_part = jnp.dot(all_rows, decay_inner_weight, preferred_element_type=jnp.float32).astype(
        jnp.bfloat16
    )
    projected = jnp.concatenate([summed.astype(jnp.bfloat16), rank_part], axis=1)
    sequence_length = projected.shape[0]
    blocks = sequence_length // BLOCK
    heads_here = qk_cols // KEY_CHANNELS
    pool_input = projected[:, :pool_cols]
    query_part = projected[:, pool_cols : pool_cols + qk_cols]
    key_part = projected[:, pool_cols + qk_cols : pool_cols + 2 * qk_cols]
    value_part = projected[:, pool_cols + 2 * qk_cols : pool_cols + 2 * qk_cols + value_cols]
    low_rank = projected[:, pool_cols + 2 * qk_cols + value_cols :]
    window = jnp.left_shift(jnp.int32(2), tp_index)
    half_width = window // 2
    padded = extended(pool_input, ((SP, 0),), rim_width)
    floats = padded.astype(jnp.float32)
    window_sum = jnp.zeros((sequence_length, pool_cols), jnp.float32)
    for offset in range(-rim_width, rim_width):
        inside = ((offset >= -half_width) & (offset < window - half_width)).astype(jnp.float32)
        window_sum = (
            window_sum + inside * floats[rim_width + offset : rim_width + offset + sequence_length]
        )
    seq_length = sequence_length * lax.axis_size(SP)
    position = sp_index * sequence_length + jnp.arange(sequence_length, dtype=jnp.int32)
    low_end = jnp.clip(position - half_width, 0, seq_length - 1)
    high_end = jnp.clip(position - half_width + window - 1, 0, seq_length - 1)
    counted = (high_end - low_end + 1).astype(jnp.float32)[:, None]
    pooled = (window_sum / counted - floats[rim_width : rim_width + sequence_length]).astype(
        jnp.bfloat16
    )
    mix_here = lax.dynamic_index_in_dim(pooling_group_map, tp_index, 0, keepdims=False)
    pool_output = jnp.dot(pooled, mix_here, preferred_element_type=jnp.float32).astype(jnp.bfloat16)

    def split_heads(token_level, width):
        return (
            token_level.astype(jnp.float32)
            .reshape(blocks, BLOCK, heads_here, width)
            .transpose(2, 0, 1, 3)
        )

    queries = split_heads(query_part, KEY_CHANNELS) * KEY_CHANNELS ** (-0.5)
    key_rows = split_heads(key_part, KEY_CHANNELS)
    value_rows = split_heads(value_part, DV)
    up_here = lax.dynamic_slice_in_dim(decay_outer_weight, tp_index * qk_cols, qk_cols, 2)
    bias_here = lax.dynamic_slice_in_dim(channel_decay_bias, tp_index * qk_cols, qk_cols, 1)
    spike_amounts = spike_log_decay.T[:, :, None]

    def log_decay(direction):
        preactivation = (
            jnp.dot(
                low_rank[:, direction * RANK : (direction + 1) * RANK],
                up_here[direction],
                preferred_element_type=jnp.float32,
            )
            + bias_here[direction]
        )
        token_level = (jax.nn.log_sigmoid(preactivation) / gate_norm_factor).reshape(
            sequence_length, heads_here, KEY_CHANNELS
        ) + spike_amounts
        return token_level.reshape(blocks, BLOCK, heads_here, KEY_CHANNELS).transpose(2, 0, 1, 3)

    cum_fwd = jnp.cumsum(log_decay(0), axis=2)
    cum_bwd = jnp.flip(jnp.cumsum(jnp.flip(log_decay(1), 2), axis=2), 2)
    scaled_fwd, inner_fwd = within_blocks(queries, cum_fwd, key_rows, value_rows, True)
    scaled_bwd, inner_bwd = within_blocks(queries, cum_bwd, key_rows, value_rows, False)
    edge_fwd = cum_fwd[:, :, -1, :]
    edge_bwd = cum_bwd[:, :, 0, :]
    updates_fwd = block_updates(key_rows, value_rows, cum_fwd, edge_fwd)
    updates_bwd = block_updates(key_rows, value_rows, cum_bwd, edge_bwd)
    total_fwd, before_fwd = local_chain(
        jnp.moveaxis(edge_fwd, 1, 0), jnp.moveaxis(updates_fwd, 1, 0), False
    )
    total_bwd, before_bwd = local_chain(
        jnp.moveaxis(edge_bwd, 1, 0), jnp.moveaxis(updates_bwd, 1, 0), True
    )
    neutral = (jnp.zeros_like(total_fwd[0]), jnp.zeros_like(total_fwd[1]))
    prefix_fwd = carried_in(total_fwd, SP, chain_combine, neutral)
    prefix_bwd = carried_in_2(total_bwd, SP, chain_combine, neutral)
    entering_fwd = jnp.exp(prefix_fwd[0])[..., None] * starting_state[0] + prefix_fwd[1]
    entering_bwd = jnp.exp(prefix_bwd[0])[..., None] * starting_state[1] + prefix_bwd[1]
    out_fwd = inner_fwd + carried_term(scaled_fwd, before_fwd, entering_fwd)
    out_bwd = inner_bwd + carried_term(scaled_bwd, before_bwd, entering_bwd)
    joined = out_fwd + out_bwd
    normal_scale = lax.rsqrt(jnp.mean(joined * joined, axis=-1, keepdims=True) + eps_value)
    attention_output = (
        (joined * normal_scale)
        .astype(jnp.bfloat16)
        .transpose(1, 2, 0, 3)
        .reshape(sequence_length, heads_here * DV)
    )
    whole_pool, whole_attention = gather_turned(
        (pooling_output_weight, attention_output_weight), SP, (1, 1)
    )
    part_one = jnp.dot(pool_output, whole_pool, preferred_element_type=jnp.float32)
    part_two = jnp.dot(attention_output, whole_attention, preferred_element_type=jnp.float32)
    mixed = sum_at_owner((part_one + part_two).astype(jnp.bfloat16), "tp", 0)
    return mixed.astype(jnp.bfloat16)


def solution(mesh):
    split = Mesh(mesh.devices.reshape(8, 8, 2, mesh.shape["tp"]), ("sp_0", "sp_1", "sp_2", "tp"))
    in_specs = (
        P(SP_TP, None),
        P(SP, "tp"),
        P(SP, "tp"),
        P(SP, "tp"),
        P(SP, "tp"),
        P(),
        P(),
        P(),
        P("tp", SP),
        P(None, "tp", None, None),
        P(),
        P("tp", SP),
        P("tp", SP),
    )
    out_specs = P(SP_TP, None)
    return jax.shard_map(
        shards, mesh=split, in_specs=in_specs, out_specs=out_specs, check_vma=False
    )
```

profile of v0, /device:TPU:2, one launch (start us, length us, event | category | flops | bytes accessed | tf_op | source)
XLA Modules:
  0.0 326.1 jit_solution(17219555616986555512)
XLA Ops:
  12.0 9.6 %all-to-all-start = ((bf16[4,128,2048]{2,1,0:T(8,128)(2,1)}), bf16[4,128,2048]{2,1,0:T(8,128)(2,1)S(1)}, u32[]{:S(2)}, u32[]{:S(2)}) async-start(bf16[4,128,2048]{2,1,0:T(8,128)(2,1)} %broadcast_in_dim.42), calls=%async_computation | async-start | bytes 4194304 | tf_op jit(solution)/shard_map/all_to_all | solution.py:20
  24.8 17.1 %all-to-all-done = bf16[4,128,2048]{2,1,0:T(8,128)(2,1)S(1)} async-done(((bf16[4,128,2048]{2,1,0:T(8,128)(2,1)}), bf16[4,128,2048]{2,1,0:T(8,128)(2,1)S(1)}, u32[]{:S(2)}, u32[]{:S(2)}) %all-to-all-start) | async-done | bytes 2097184 | tf_op jit(solution)/shard_map/all_to_all | solution.py:20
  46.8 1.9 rev.7
  51.6 2.1 reshape.1391
  56.3 42.6 %all-gather.12.cloned.1.call-done = bf16[2048,768]{1,0:T(8,128)(2,1)} async-done(((bf16[16,768]{1,0:T(8,128)(2,1)}), bf16[2048,768]{1,0:T(8,128)(2,1)}) %all-gather.12.cloned.1.call-update) | async-done | bytes 3145744 | tf_op jit(solution)/shard_map/all_gather | solution.py:211
  98.9 3.7 %convolution_convert_fusion = bf16[512,768]{1,0:T(8,128)(2,1)S(1)} fusion(bf16[512,2048]{1,0:T(8,128)(2,1)S(1)} %bitcast.287, bf16[2048,768]{1,0:T(8,128)(2,1)} %all-gather.12.cloned.1.call-done), kind=kOutput, calls=%fused_computation.13 | convolution fusion | flops 1611005952 | bytes 6029312 | tf_op jit(solution)/shard_map/dot_general | solution.py:209
  105.5 2.8 bitcast_multiply_fusion.1
  108.6 7.0 %while.39 = (s32[]{:T(128)}, f32[2,64]{1,0:T(2,128)S(1)}, f32[2,64,128]{2,1,0:T(8,128)S(1)}, f32[8,2,64]{2,1,0:T(2,128)S(1)}, f32[8,2,64,128]{3,2,1,0:T(8,128)S(...) while((s32[]{:T(128)}, f32[2,64]{1,0:T(2,128)S(1)}, ...), condition=%wide.region_6.7_spmd.clone, body=%wide.region_5.6_spmd.clone.sunk | while | flops 65924 | bytes 333454 | solution.py:159
  115.7 1.8 all-gather.6
  117.7 24.9 %all-gather.7 = bf16[8,129,128]{2,1,0:T(8,128)(2,1)S(1)} all-gather(bf16[1,129,128]{2,1,0:T(8,128)(2,1)S(1)} %maximum_bitcast_fusion.1), channel_id=5, replica_groups=mesh['sp_0'=8,'sp_1'=8,'sp_2'=2,'tp'=4] {'sp_1'}, dimensions={0}, use_global_device_ids=true | all-gather | bytes 297216 | tf_op jit(solution)/shard_map/all_gather | solution.py:82
  142.9 25.0 %all-gather.8 = bf16[8,129,128]{2,1,0:T(8,128)(2,1)S(1)} all-gather(bf16[1,129,128]{2,1,0:T(8,128)(2,1)S(1)} %maximum_bitcast_fusion.2), channel_id=6, replica_groups=mesh['sp_0'=8,'sp_1'=8,'sp_2'=2,'tp'=4] {'sp_0'}, dimensions={0}, use_global_device_ids=true | all-gather | bytes 297216 | tf_op jit(solution)/shard_map/all_gather | solution.py:82
  181.8 7.0 %while.38 = (s32[]{:T(128)}, f32[2,64]{1,0:T(2,128)S(1)}, f32[2,64,128]{2,1,0:T(8,128)S(1)}, f32[8,2,64]{2,1,0:T(2,128)S(1)}, f32[8,2,64,128]{3,2,1,0:T(8,128)S(...) while((s32[]{:T(128)}, f32[2,64]{1,0:T(2,128)S(1)}, ...), condition=%wide.region_3.4_spmd.clone, body=%wide.region_2.3_spmd.clone.sunk | while | flops 65923 | bytes 333434 | solution.py:159
  189.0 1.8 all-gather.5
  190.8 15.0 %all_gather.56 = bf16[8,2,64]{2,1,0:T(2,128)(2,1)S(1)} all-gather(bf16[1,2,64]{2,1,0:T(2,128)(2,1)S(1)} %get-tuple-element.410), channel_id=1, replica_groups=mesh['sp_0'=8,'sp_1'=8,'sp_2'=2,'tp'=4] {'sp_1'}, dimensions={0}, use_global_device_ids=true | all-gather | bytes 2304 | tf_op jit(solution)/shard_map/all_gather | solution.py:59
  205.9 14.8 %all_gather.57 = bf16[8,2,64]{2,1,0:T(2,128)(2,1)S(1)} all-gather(bf16[1,2,64]{2,1,0:T(2,128)(2,1)S(1)} %get-tuple-element.398), channel_id=1, replica_groups=mesh['sp_0'=8,'sp_1'=8,'sp_2'=2,'tp'=4] {'sp_0'}, dimensions={0}, use_global_device_ids=true | all-gather | bytes 2304 | tf_op jit(solution)/shard_map/all_gather | solution.py:59
  220.7 1.8 all-gather.1
  222.5 2.1 collective-permute-start
  226.0 28.0 %all_gather.60 = bf16[8,2,64,128]{3,2,1,0:T(8,128)(2,1)S(1)} all-gather(bf16[1,2,64,128]{3,2,1,0:T(8,128)(2,1)S(1)} %fusion.138), channel_id=1, replica_groups=mesh['sp_0'=8,'sp_1'=8,'sp_2'=2,'tp'=4] {'sp_1'}, dimensions={0}, use_global_device_ids=true | all-gather | bytes 294912 | tf_op jit(solution)/shard_map/all_gather | solution.py:59
  254.2 26.6 %all_gather.61 = bf16[8,2,64,128]{3,2,1,0:T(8,128)(2,1)S(1)} all-gather(bf16[1,2,64,128]{3,2,1,0:T(8,128)(2,1)S(1)} %fusion.137), channel_id=1, replica_groups=mesh['sp_0'=8,'sp_1'=8,'sp_2'=2,'tp'=4] {'sp_0'}, dimensions={0}, use_global_device_ids=true | all-gather | bytes 294912 | tf_op jit(solution)/shard_map/all_gather | solution.py:59
  281.7 1.9 fusion.126
  285.7 2.1 fusion.3
  290.3 5.1 %fusion.5 = f32[512,2048]{1,0:T(8,128)} fusion(bf16[2048,512]{1,0:T(8,128)(2,1)} %all-gather.14.cloned.1.call-done, f32[528,256]{1,0:T(8,128)S(1)} %maximum_convert_fusion, f32[512]{0:T(512)S(1)} %copy-done.15, f32[]{:T(128)S(6)} %convert_element_type.1186, f32[]{:T(128)S(6)} %convert_element_type.1185, f32[]{:T(128)S(6)} %convert_element_type.1184, ...), kind=kOutput, calls=%fused_computation.26 | convolution fusion | flops 608567296 | bytes 13764676 | tf_op jit(solution)/shard_map/dot_general | solution.py:307
  295.4 2.9 add_convert_fusion
  298.3 19.7 %all_to_all.10 = bf16[4,128,2048]{2,1,0:T(8,128)(2,1)S(1)} all-to-all(bf16[4,128,2048]{2,1,0:T(8,128)(2,1)S(1)} %bitcast.288), channel_id=1, replica_groups=mesh['sp_0'=8,'sp_1'=8,'sp_2'=2,'tp'=4] {'tp'}, dimensions={0} | all-to-all | bytes 4194304 | tf_op jit(solution)/shard_map/all_to_all | solution.py:134
  (258 shorter events, 57.8 us)
Async XLA Ops:
  6.5 283.8 %copy-start = (bf16[4,256,256]{2,1,0:T(8,128)(2,1)S(1)}, bf16[4,256,256]{2,1,0:T(8,128)(2,1)}, u32[]{:S(2)}) copy-start(bf16[4,256,256]{2,1,0:T(8,128)(2,1)} %param.27) | copy-start | bytes 1572868
  6.5 92.3 %all-gather.12.cloned.1.call-start = ((), (), s32[]{:S(2)}) async-start(), calls=%async_computation.2 | async-start | bytes 3170304 | tf_op jit(solution)/shard_map/all_gather | solution.py:211
  12.0 29.8 %all-to-all-start = ((bf16[4,128,2048]{2,1,0:T(8,128)(2,1)}), bf16[4,128,2048]{2,1,0:T(8,128)(2,1)S(1)}, u32[]{:S(2)}, u32[]{:S(2)}) async-start(bf16[4,128,2048]{2,1,0:T(8,128)(2,1)} %broadcast_in_dim.42), calls=%async_computation | async-start | bytes 4194304 | tf_op jit(solution)/shard_map/all_to_all | solution.py:20
  21.6 268.7 %all-gather.14.cloned.1.call-start = ((), (), s32[]{:S(2)}) async-start(), calls=%async_computation.3 | async-start | bytes 2113536 | tf_op jit(solution)/shard_map/all_gather | solution.py:118
  188.8 94.9 %copy-start.8 = (f32[2,2,64,128]{3,2,1,0:T(8,128)S(1)}, f32[2,2,64,128]{3,2,1,0:T(8,128)}, u32[]{:S(2)}) copy-start(f32[2,2,64,128]{3,2,1,0:T(8,128)} %param.26) | copy-start | bytes 393220
  188.8 94.9 %copy-start.16 = (f32[2,64]{1,0:T(2,128)S(1)}, f32[2,64]{1,0:T(2,128)}, u32[]{:S(2)}) copy-start(f32[2,64]{1,0:T(2,128)} %reshape.1519) | copy-start | bytes 1540
  188.8 94.9 %copy-start.17 = (f32[2,64]{1,0:T(2,128)S(1)}, f32[2,64]{1,0:T(2,128)}, u32[]{:S(2)}) copy-start(f32[2,64]{1,0:T(2,128)} %reshape.1557) | copy-start | bytes 1540
  188.8 94.9 %copy-start.18 = (f32[2,64]{1,0:T(2,128)S(1)}, f32[2,64]{1,0:T(2,128)}, u32[]{:S(2)}) copy-start(f32[2,64]{1,0:T(2,128)} %reshape.1568) | copy-start | bytes 1540
  188.8 94.9 %copy-start.19 = (f32[2,64]{1,0:T(2,128)S(1)}, f32[2,64]{1,0:T(2,128)}, u32[]{:S(2)}) copy-start(f32[2,64]{1,0:T(2,128)} %exp.501) | copy-start | bytes 1540
  188.8 94.9 %copy-start.20 = (f32[2,64]{1,0:T(2,128)S(1)}, f32[2,64]{1,0:T(2,128)}, u32[]{:S(2)}) copy-start(f32[2,64]{1,0:T(2,128)} %exp.503) | copy-start | bytes 1540
  188.9 94.9 %copy-start.21 = (f32[2,64]{1,0:T(2,128)S(1)}, f32[2,64]{1,0:T(2,128)}, u32[]{:S(2)}) copy-start(f32[2,64]{1,0:T(2,128)} %exp.505) | copy-start | bytes 1540
  188.9 94.9 %copy-start.22 = (f32[2,64]{1,0:T(2,128)S(1)}, f32[2,64]{1,0:T(2,128)}, u32[]{:S(2)}) copy-start(f32[2,64]{1,0:T(2,128)} %mul.911) | copy-start | bytes 1540
  188.9 94.9 %copy-start.23 = (f32[2,64]{1,0:T(2,128)S(1)}, f32[2,64]{1,0:T(2,128)}, u32[]{:S(2)}) copy-start(f32[2,64]{1,0:T(2,128)} %reshape.1462) | copy-start | bytes 1540
  188.9 94.9 %copy-start.24 = (f32[2,64]{1,0:T(2,128)S(1)}, f32[2,64]{1,0:T(2,128)}, u32[]{:S(2)}) copy-start(f32[2,64]{1,0:T(2,128)} %reshape.1480) | copy-start | bytes 1540
  188.9 94.9 %copy-start.25 = (f32[2,64]{1,0:T(2,128)S(1)}, f32[2,64]{1,0:T(2,128)}, u32[]{:S(2)}) copy-start(f32[2,64]{1,0:T(2,128)} %reshape.1497) | copy-start | bytes 1540
  188.9 94.9 %copy-start.26 = (f32[2,64]{1,0:T(2,128)S(1)}, f32[2,64]{1,0:T(2,128)}, u32[]{:S(2)}) copy-start(f32[2,64]{1,0:T(2,128)} %exp.512) | copy-start | bytes 1540
  188.9 94.9 %copy-start.27 = (f32[2,64]{1,0:T(2,128)S(1)}, f32[2,64]{1,0:T(2,128)}, u32[]{:S(2)}) copy-start(f32[2,64]{1,0:T(2,128)} %exp.513) | copy-start | bytes 1540
  188.9 94.9 %copy-start.28 = (f32[2,64]{1,0:T(2,128)S(1)}, f32[2,64]{1,0:T(2,128)}, u32[]{:S(2)}) copy-start(f32[2,64]{1,0:T(2,128)} %exp.514) | copy-start | bytes 1540
  188.9 94.9 %copy-start.29 = (f32[2,64]{1,0:T(2,128)S(1)}, f32[2,64]{1,0:T(2,128)}, u32[]{:S(2)}) copy-start(f32[2,64]{1,0:T(2,128)} %mul.929) | copy-start | bytes 1540
  188.9 94.9 %copy-start.30 = (f32[2,64]{1,0:T(2,128)S(1)}, f32[2,64]{1,0:T(2,128)}, u32[]{:S(2)}) copy-start(f32[2,64]{1,0:T(2,128)} %reshape.1463) | copy-start | bytes 1540
  189.0 94.9 %copy-start.31 = (f32[2,64]{1,0:T(2,128)S(1)}, f32[2,64]{1,0:T(2,128)}, u32[]{:S(2)}) copy-start(f32[2,64]{1,0:T(2,128)} %reshape.1481) | copy-start | bytes 1540
  189.0 94.9 %copy-start.32 = (f32[2,64]{1,0:T(2,128)S(1)}, f32[2,64]{1,0:T(2,128)}, u32[]{:S(2)}) copy-start(f32[2,64]{1,0:T(2,128)} %reshape.1498) | copy-start | bytes 1540
  222.5 67.7 %collective-permute-start = (bf16[8,256]{1,0:T(8,128)(2,1)}, bf16[8,256]{1,0:T(8,128)(2,1)S(1)}, u32[]{:S(2)}, u32[]{:S(2)}) collective-permute-start(bf16[8,256]{1,0:T(8,128)(2,1)} %get-tuple-element.350), channel_id=1, source_target_pairs={{0,4},{4,8},{8,12},{12,16},{16,20},{20,24},{24,28},{28,32},{32,36}... | collective-permute-start | bytes 12296 | tf_op jit(solution)/shard_map/ppermute | solution.py:41
  224.6 65.6 %collective-permute-start.1 = (bf16[8,256]{1,0:T(8,128)(2,1)}, bf16[8,256]{1,0:T(8,128)(2,1)S(1)}, u32[]{:S(2)}, u32[]{:S(2)}) collective-permute-start(bf16[8,256]{1,0:T(8,128)(2,1)} %get-tuple-element.351), channel_id=1, source_target_pairs={{4,0},{8,4},{12,8},{16,12},{20,16},{24,20},{28,24},{32,28},{36,32}... | collective-permute-start | bytes 12296 | tf_op jit(solution)/shard_map/ppermute | solution.py:42
  (18 other events, 554.5 us)
Sparse Core Ops, SparseCore 0:
  10.5 88.3 all-gather.11
  102.0 80.1 all-gather.13
where the time goes:
time: 328 us; the launch traced here: 326 us
  blocking collectives  159 us (48%)
  waiting for transfers between devices  59.8 us (18%)
  local copies, waits for them, and re-layouts  37.4 us (11%)
  matrix products  21.7 us (7%)
  other arithmetic  19.6 us (6%)
  between operations  14.6 us (4%)
  starting transfers between devices  13 us (4%)
    all_gather x6, blocking collectives, carried_in(): lax.all_gather(part.astype(kind), axis)  88 us
    all_gather x3, blocking collectives, gathered_once(): both, at, found = (lax.all_gather(jnp.concatenate(lines), axis), 0, {})  51.7 us
    all_gather x1, waiting for transfers between devices, shards(): lax.all_gather(local_weight, SP, axis=0, tiled=True)  42.6 us
    all_to_all x1, blocking collectives, sum_at_owner(): lax.all_to_all(cut_along(value, dim, devices), axis, 0, 0, tiled=True)  19.7 us
    all_to_all x1, waiting for transfers between devices, from_everyone(): return lax.all_to_all(copies, axis, split_axis=0, concat_axis=0, tiled=True)  17.1 us
    dynamic_slice x16, local copies, waits for them, and re-layouts, local_chain(): return lax.scan(advance, begin, (decays, updates), reverse=backward)  11.3 us
    exp x19, local copies, waits for them, and re-layouts, chain_combine(): jnp.exp(later[0])[..., None] * earlier[1] + later[1]  11 us
    all_to_all x1, starting transfers between devices, from_everyone(): return lax.all_to_all(copies, axis, split_axis=0, concat_axis=0, tiled=True)  9.6 us
  transfers between devices with their start and end apart: 5, of which 2 were waited for; matrix products, arithmetic and copies ran while one was open for 21% of the time, Pallas kernels for 0%

commit v1 on v0

--- a/solution.py
+++ b/solution.py
@@ -208,7 +208,9 @@
     all_rows = gathered_copies(normed, "tp", 0)
     summed = jnp.dot(
         all_rows,
-        lax.all_gather(local_weight, SP, axis=0, tiled=True),
+        jnp.concatenate(
+            lax.all_to_all(jnp.stack([local_weight] * lax.axis_size(SP)), SP, 0, 0), axis=0
+        ),
         preferred_element_type=jnp.float32,
     )
     rank_part = jnp.dot(all_rows, decay_inner_weight, preferred_element_type=jnp.float32).astype(

time: 328 us -> 363 us (1.11)
  waiting for transfers between devices: 59.8 us -> 78.2 us
  starting transfers between devices: 13 us -> 31.4 us
    all_to_all x0 -> x1, waiting for transfers between devices: none -> 57.9 us  [shards(): lax.all_to_all(jnp.stack([local_weight] * lax.axis_size(SP)), SP, 0, 0)]
    all_gather x1 -> x0, waiting for transfers between devices: 42.6 us -> none  [shards(): lax.all_gather(local_weight, SP, axis=0, tiled=True)]
    all_to_all x0 -> x1, starting transfers between devices: none -> 18.4 us  [shards(): lax.all_to_all(jnp.stack([local_weight] * lax.axis_size(SP)), SP, 0, 0)]
  transfers between devices with their start and end apart: 5 -> 5, of which waited for: 2 -> 2; matrix products, arithmetic and copies ran while one was open for 21% -> 17% of each run, Pallas kernels for 0% -> 0%
where the time goes in v1:
time: 363 us; the launch traced here: 361 us
  blocking collectives  159 us (44%)
  waiting for transfers between devices  78.2 us (22%)
  local copies, waits for them, and re-layouts  38.4 us (11%)
  starting transfers between devices  31.4 us (9%)
  matrix products  20.9 us (6%)
  other arithmetic  18.3 us (5%)
  between operations  14.7 us (4%)
    all_gather x6, blocking collectives, carried_in(): lax.all_gather(part.astype(kind), axis)  87.6 us
    all_to_all x1, waiting for transfers between devices, shards(): lax.all_to_all(jnp.stack([local_weight] * lax.axis_size(SP)), SP, 0, 0)  57.9 us
    all_gather x3, blocking collectives, gathered_once(): both, at, found = (lax.all_gather(jnp.concatenate(lines), axis), 0, {})  52.3 us
    all_to_all x1, waiting for transfers between devices, from_everyone(): return lax.all_to_all(copies, axis, split_axis=0, concat_axis=0, tiled=True)  20.2 us
    all_to_all x1, blocking collectives, sum_at_owner(): lax.all_to_all(cut_along(value, dim, devices), axis, 0, 0, tiled=True)  19.1 us
    all_to_all x1, starting transfers between devices, shards(): lax.all_to_all(jnp.stack([local_weight] * lax.axis_size(SP)), SP, 0, 0)  18.4 us
    dynamic_slice x16, local copies, waits for them, and re-layouts, local_chain(): return lax.scan(advance, begin, (decays, updates), reverse=backward)  11.3 us
    exp x19, local copies, waits for them, and re-layouts, chain_combine(): jnp.exp(later[0])[..., None] * earlier[1] + later[1]  10.9 us
  transfers between devices with their start and end apart: 5, of which 2 were waited for; matrix products, arithmetic and copies ran while one was open for 17% of the time, Pallas kernels for 0%

profile of v1, /device:TPU:2, one launch (start us, length us, event | category | flops | bytes accessed | tf_op | source)
XLA Modules:
  0.0 361.4 jit_solution(13412414644414750431)
XLA Ops:
  10.7 9.6 %all-to-all-start = ((bf16[4,128,2048]{2,1,0:T(8,128)(2,1)}), bf16[4,128,2048]{2,1,0:T(8,128)(2,1)S(1)}, u32[]{:S(2)}, u32[]{:S(2)}) async-start(bf16[4,128,2048]{2,1,0:T(8,128)(2,1)} %broadcast_in_dim.42), calls=%async_computation | async-start | bytes 4194304 | tf_op jit(solution)/shard_map/all_to_all | solution.py:20
  20.3 20.2 %all-to-all-done = bf16[4,128,2048]{2,1,0:T(8,128)(2,1)S(1)} async-done(((bf16[4,128,2048]{2,1,0:T(8,128)(2,1)}), bf16[4,128,2048]{2,1,0:T(8,128)(2,1)S(1)}, u32[]{:S(2)}, u32[]{:S(2)}) %all-to-all-start) | async-done | bytes 2097184 | tf_op jit(solution)/shard_map/all_to_all | solution.py:20
  40.5 1.9 stack.2
  42.4 18.4 %all-to-all-start.1 = ((bf16[128,16,768]{2,1,0:T(8,128)(2,1)}), bf16[128,16,768]{2,1,0:T(8,128)(2,1)}, u32[]{:S(2)}, u32[]{:S(2)}) async-start(bf16[128,16,768]{2,1,0:T(8,128)(2,1)} %stack.2), calls=%async_computation.1 | async-start | bytes 6291456 | tf_op jit(solution)/shard_map/all_to_all | solution.py:212
  68.9 1.9 rev.7
  76.8 57.9 %all-to-all-done.1 = bf16[128,16,768]{2,1,0:T(8,128)(2,1)} async-done(((bf16[128,16,768]{2,1,0:T(8,128)(2,1)}), bf16[128,16,768]{2,1,0:T(8,128)(2,1)}, u32[]{:S(2)}, u32[]{:S(2)}) %all-to-all-start.1) | async-done | bytes 3145760 | tf_op jit(solution)/shard_map/all_to_all | solution.py:212
  134.7 3.7 %convolution_convert_fusion = bf16[512,768]{1,0:T(8,128)(2,1)S(1)} fusion(bf16[512,2048]{1,0:T(8,128)(2,1)S(1)} %bitcast.288, bf16[2048,768]{1,0:T(8,128)(2,1)} %bitcast.1), kind=kOutput, calls=%fused_computation.13 | convolution fusion | flops 1611005952 | bytes 6029312 | tf_op jit(solution)/shard_map/dot_general | solution.py:209
  141.4 2.8 bitcast_multiply_fusion.1
  144.5 7.0 %while.39 = (s32[]{:T(128)}, f32[2,64]{1,0:T(2,128)S(1)}, f32[2,64,128]{2,1,0:T(8,128)S(1)}, f32[8,2,64]{2,1,0:T(2,128)S(1)}, f32[8,2,64,128]{3,2,1,0:T(8,128)S(...) while((s32[]{:T(128)}, f32[2,64]{1,0:T(2,128)S(1)}, ...), condition=%wide.region_6.7_spmd.clone, body=%wide.region_5.6_spmd.clone.sunk | while | flops 65924 | bytes 333454 | solution.py:159
  151.6 1.8 all-gather.6
  153.6 25.6 %all-gather.7 = bf16[8,129,128]{2,1,0:T(8,128)(2,1)S(1)} all-gather(bf16[1,129,128]{2,1,0:T(8,128)(2,1)S(1)} %maximum_bitcast_fusion.1), channel_id=5, replica_groups=mesh['sp_0'=8,'sp_1'=8,'sp_2'=2,'tp'=4] {'sp_1'}, dimensions={0}, use_global_device_ids=true | all-gather | bytes 297216 | tf_op jit(solution)/shard_map/all_gather | solution.py:82
  179.4 24.9 %all-gather.8 = bf16[8,129,128]{2,1,0:T(8,128)(2,1)S(1)} all-gather(bf16[1,129,128]{2,1,0:T(8,128)(2,1)S(1)} %maximum_bitcast_fusion.2), channel_id=6, replica_groups=mesh['sp_0'=8,'sp_1'=8,'sp_2'=2,'tp'=4] {'sp_0'}, dimensions={0}, use_global_device_ids=true | all-gather | bytes 297216 | tf_op jit(solution)/shard_map/all_gather | solution.py:82
  218.2 7.0 %while.38 = (s32[]{:T(128)}, f32[2,64]{1,0:T(2,128)S(1)}, f32[2,64,128]{2,1,0:T(8,128)S(1)}, f32[8,2,64]{2,1,0:T(2,128)S(1)}, f32[8,2,64,128]{3,2,1,0:T(8,128)S(...) while((s32[]{:T(128)}, f32[2,64]{1,0:T(2,128)S(1)}, ...), condition=%wide.region_3.4_spmd.clone, body=%wide.region_2.3_spmd.clone.sunk | while | flops 65923 | bytes 333434 | solution.py:159
  227.2 16.5 %all_gather.52 = bf16[8,2,64]{2,1,0:T(2,128)(2,1)S(1)} all-gather(bf16[1,2,64]{2,1,0:T(2,128)(2,1)S(1)} %get-tuple-element.410), channel_id=1, replica_groups=mesh['sp_0'=8,'sp_1'=8,'sp_2'=2,'tp'=4] {'sp_1'}, dimensions={0}, use_global_device_ids=true | all-gather | bytes 2304 | tf_op jit(solution)/shard_map/all_gather | solution.py:59
  243.8 14.7 %all_gather.53 = bf16[8,2,64]{2,1,0:T(2,128)(2,1)S(1)} all-gather(bf16[1,2,64]{2,1,0:T(2,128)(2,1)S(1)} %get-tuple-element.398), channel_id=1, replica_groups=mesh['sp_0'=8,'sp_1'=8,'sp_2'=2,'tp'=4] {'sp_0'}, dimensions={0}, use_global_device_ids=true | all-gather | bytes 2304 | tf_op jit(solution)/shard_map/all_gather | solution.py:59
  258.5 1.8 all-gather.1
  260.3 2.1 collective-permute-start
  263.8 26.5 %all_gather.56 = bf16[8,2,64,128]{3,2,1,0:T(8,128)(2,1)S(1)} all-gather(bf16[1,2,64,128]{3,2,1,0:T(8,128)(2,1)S(1)} %fusion.138), channel_id=1, replica_groups=mesh['sp_0'=8,'sp_1'=8,'sp_2'=2,'tp'=4] {'sp_1'}, dimensions={0}, use_global_device_ids=true | all-gather | bytes 294912 | tf_op jit(solution)/shard_map/all_gather | solution.py:59
  290.5 26.2 %all_gather.57 = bf16[8,2,64,128]{3,2,1,0:T(8,128)(2,1)S(1)} all-gather(bf16[1,2,64,128]{3,2,1,0:T(8,128)(2,1)S(1)} %fusion.137), channel_id=1, replica_groups=mesh['sp_0'=8,'sp_1'=8,'sp_2'=2,'tp'=4] {'sp_0'}, dimensions={0}, use_global_device_ids=true | all-gather | bytes 294912 | tf_op jit(solution)/shard_map/all_gather | solution.py:59
  317.6 1.9 fusion.126
  321.6 2.1 fusion.3
  326.2 4.9 %fusion.5 = f32[512,2048]{1,0:T(8,128)} fusion(bf16[2048,512]{1,0:T(8,128)(2,1)} %all-gather.11.cloned.1.call-done, f32[528,256]{1,0:T(8,128)S(1)} %maximum_convert_fusion, f32[512]{0:T(512)S(1)} %copy-done.19, f32[]{:T(128)S(6)} %convert_element_type.1186, f32[]{:T(128)S(6)} %convert_element_type.1185, f32[]{:T(128)S(6)} %convert_element_type.1184, ...), kind=kOutput, calls=%fused_computation.26 | convolution fusion | flops 608567296 | bytes 13764676 | tf_op jit(solution)/shard_map/dot_general | solution.py:309
  331.2 2.9 add_convert_fusion
  334.1 19.1 %all_to_all.15 = bf16[4,128,2048]{2,1,0:T(8,128)(2,1)S(1)} all-to-all(bf16[4,128,2048]{2,1,0:T(8,128)(2,1)S(1)} %bitcast.289), channel_id=1, replica_groups=mesh['sp_0'=8,'sp_1'=8,'sp_2'=2,'tp'=4] {'tp'}, dimensions={0} | all-to-all | bytes 4194304 | tf_op jit(solution)/shard_map/all_to_all | solution.py:134
  (266 shorter events, 58.5 us)
Async XLA Ops:
  6.5 319.7 %copy-start = (bf16[4,256,256]{2,1,0:T(8,128)(2,1)S(1)}, bf16[4,256,256]{2,1,0:T(8,128)(2,1)}, u32[]{:S(2)}) copy-start(bf16[4,256,256]{2,1,0:T(8,128)(2,1)} %param.27) | copy-start | bytes 1572868
  10.7 29.8 %all-to-all-start = ((bf16[4,128,2048]{2,1,0:T(8,128)(2,1)}), bf16[4,128,2048]{2,1,0:T(8,128)(2,1)S(1)}, u32[]{:S(2)}, u32[]{:S(2)}) async-start(bf16[4,128,2048]{2,1,0:T(8,128)(2,1)} %broadcast_in_dim.42), calls=%async_computation | async-start | bytes 4194304 | tf_op jit(solution)/shard_map/all_to_all | solution.py:20
  42.4 92.3 %all-to-all-start.1 = ((bf16[128,16,768]{2,1,0:T(8,128)(2,1)}), bf16[128,16,768]{2,1,0:T(8,128)(2,1)}, u32[]{:S(2)}, u32[]{:S(2)}) async-start(bf16[128,16,768]{2,1,0:T(8,128)(2,1)} %stack.2), calls=%async_computation.1 | async-start | bytes 6291456 | tf_op jit(solution)/shard_map/all_to_all | solution.py:212
  60.8 265.4 %all-gather.11.cloned.1.call-start = ((), (), s32[]{:S(2)}) async-start(), calls=%async_computation.3 | async-start | bytes 2113536 | tf_op jit(solution)/shard_map/all_gather | solution.py:118
  225.1 94.4 %copy-start.8 = (f32[2,2,64,128]{3,2,1,0:T(8,128)S(1)}, f32[2,2,64,128]{3,2,1,0:T(8,128)}, u32[]{:S(2)}) copy-start(f32[2,2,64,128]{3,2,1,0:T(8,128)} %param.26) | copy-start | bytes 393220
  225.2 94.4 %copy-start.20 = (f32[2,64]{1,0:T(2,128)S(1)}, f32[2,64]{1,0:T(2,128)}, u32[]{:S(2)}) copy-start(f32[2,64]{1,0:T(2,128)} %reshape.1525) | copy-start | bytes 1540
  225.2 94.4 %copy-start.21 = (f32[2,64]{1,0:T(2,128)S(1)}, f32[2,64]{1,0:T(2,128)}, u32[]{:S(2)}) copy-start(f32[2,64]{1,0:T(2,128)} %reshape.1563) | copy-start | bytes 1540
  225.2 94.4 %copy-start.22 = (f32[2,64]{1,0:T(2,128)S(1)}, f32[2,64]{1,0:T(2,128)}, u32[]{:S(2)}) copy-start(f32[2,64]{1,0:T(2,128)} %reshape.1574) | copy-start | bytes 1540
  225.2 94.4 %copy-start.23 = (f32[2,64]{1,0:T(2,128)S(1)}, f32[2,64]{1,0:T(2,128)}, u32[]{:S(2)}) copy-start(f32[2,64]{1,0:T(2,128)} %exp.501) | copy-start | bytes 1540
  225.2 94.4 %copy-start.24 = (f32[2,64]{1,0:T(2,128)S(1)}, f32[2,64]{1,0:T(2,128)}, u32[]{:S(2)}) copy-start(f32[2,64]{1,0:T(2,128)} %exp.503) | copy-start | bytes 1540
  225.2 94.4 %copy-start.25 = (f32[2,64]{1,0:T(2,128)S(1)}, f32[2,64]{1,0:T(2,128)}, u32[]{:S(2)}) copy-start(f32[2,64]{1,0:T(2,128)} %exp.505) | copy-start | bytes 1540
  225.2 94.4 %copy-start.26 = (f32[2,64]{1,0:T(2,128)S(1)}, f32[2,64]{1,0:T(2,128)}, u32[]{:S(2)}) copy-start(f32[2,64]{1,0:T(2,128)} %mul.911) | copy-start | bytes 1540
  225.2 94.4 %copy-start.27 = (f32[2,64]{1,0:T(2,128)S(1)}, f32[2,64]{1,0:T(2,128)}, u32[]{:S(2)}) copy-start(f32[2,64]{1,0:T(2,128)} %reshape.1468) | copy-start | bytes 1540
  225.2 94.4 %copy-start.28 = (f32[2,64]{1,0:T(2,128)S(1)}, f32[2,64]{1,0:T(2,128)}, u32[]{:S(2)}) copy-start(f32[2,64]{1,0:T(2,128)} %reshape.1486) | copy-start | bytes 1540
  225.2 94.4 %copy-start.29 = (f32[2,64]{1,0:T(2,128)S(1)}, f32[2,64]{1,0:T(2,128)}, u32[]{:S(2)}) copy-start(f32[2,64]{1,0:T(2,128)} %reshape.1503) | copy-start | bytes 1540
  225.3 94.4 %copy-start.30 = (f32[2,64]{1,0:T(2,128)S(1)}, f32[2,64]{1,0:T(2,128)}, u32[]{:S(2)}) copy-start(f32[2,64]{1,0:T(2,128)} %exp.512) | copy-start | bytes 1540
  225.3 94.4 %copy-start.31 = (f32[2,64]{1,0:T(2,128)S(1)}, f32[2,64]{1,0:T(2,128)}, u32[]{:S(2)}) copy-start(f32[2,64]{1,0:T(2,128)} %exp.513) | copy-start | bytes 1540
  225.3 94.4 %copy-start.32 = (f32[2,64]{1,0:T(2,128)S(1)}, f32[2,64]{1,0:T(2,128)}, u32[]{:S(2)}) copy-start(f32[2,64]{1,0:T(2,128)} %exp.514) | copy-start | bytes 1540
  225.3 94.4 %copy-start.33 = (f32[2,64]{1,0:T(2,128)S(1)}, f32[2,64]{1,0:T(2,128)}, u32[]{:S(2)}) copy-start(f32[2,64]{1,0:T(2,128)} %mul.929) | copy-start | bytes 1540
  225.3 94.4 %copy-start.34 = (f32[2,64]{1,0:T(2,128)S(1)}, f32[2,64]{1,0:T(2,128)}, u32[]{:S(2)}) copy-start(f32[2,64]{1,0:T(2,128)} %reshape.1469) | copy-start | bytes 1540
  225.3 94.4 %copy-start.35 = (f32[2,64]{1,0:T(2,128)S(1)}, f32[2,64]{1,0:T(2,128)}, u32[]{:S(2)}) copy-start(f32[2,64]{1,0:T(2,128)} %reshape.1487) | copy-start | bytes 1540
  225.3 94.4 %copy-start.36 = (f32[2,64]{1,0:T(2,128)S(1)}, f32[2,64]{1,0:T(2,128)}, u32[]{:S(2)}) copy-start(f32[2,64]{1,0:T(2,128)} %reshape.1504) | copy-start | bytes 1540
  260.3 65.8 %collective-permute-start = (bf16[8,256]{1,0:T(8,128)(2,1)}, bf16[8,256]{1,0:T(8,128)(2,1)S(1)}, u32[]{:S(2)}, u32[]{:S(2)}) collective-permute-start(bf16[8,256]{1,0:T(8,128)(2,1)} %get-tuple-element.350), channel_id=1, source_target_pairs={{0,4},{4,8},{8,12},{12,16},{16,20},{20,24},{24,28},{28,32},{32,36}... | collective-permute-start | bytes 12296 | tf_op jit(solution)/shard_map/ppermute | solution.py:41
  262.4 63.7 %collective-permute-start.1 = (bf16[8,256]{1,0:T(8,128)(2,1)}, bf16[8,256]{1,0:T(8,128)(2,1)S(1)}, u32[]{:S(2)}, u32[]{:S(2)}) collective-permute-start(bf16[8,256]{1,0:T(8,128)(2,1)} %get-tuple-element.351), channel_id=1, source_target_pairs={{4,0},{8,4},{12,8},{16,12},{20,16},{24,20},{28,24},{32,28},{36,32}... | collective-permute-start | bytes 12296 | tf_op jit(solution)/shard_map/ppermute | solution.py:42
  (22 other events, 609.5 us)
Sparse Core Ops, SparseCore 0:
  64.8 124.9 all-gather.10
